TPU v7x, 32 devices: a whole 2x2x4 slice. The times are simulated.
32 devices in a mesh: dp: 2 (over x), kv: 8 (over z, y), tp: 2 (over core).
Axes of the slice: x: 2, y: 2, z: 4, core: 2. Of those that a mesh axis runs over, the one named last changes fastest.
Arguments:
- tokens: bfloat16 [32, 3072], P(('tp', 'dp'), 'kv'), parts along dimension 0, may hold values from -60 to 60
- old_state: float32 [32, 24, 128, 128], P(('tp', 'dp', 'kv')), parts along dimension 0, may hold values from -0.6 to 0.6
- mixer_gain: float32 [3072], replicated, may hold values from 0.1 to 1.9
- w_query: bfloat16 [3072, 3072], P(None, 'kv'), may hold values from -0.109375 to 0.109375
- w_key: bfloat16 [3072, 3072], P(None, 'kv'), may hold values from -0.109375 to 0.109375
- w_value: bfloat16 [3072, 3072], P(None, 'kv'), may hold values from -0.109375 to 0.109375
- w_outgate: bfloat16 [3072, 3072], P(None, 'kv'), may hold values from -0.109375 to 0.109375
- w_decay: bfloat16 [3072, 24], replicated, may hold values from -0.109375 to 0.109375
- w_write: bfloat16 [3072, 24], replicated, may hold values from -0.109375 to 0.109375
- decay_log: float32 [24], replicated, may hold values from -3 to 1
- decay_bias: float32 [24], replicated, may hold values from -3 to 3
- head_gain: float32 [128], replicated, may hold values from 0.1 to 1.9
- w_output: bfloat16 [3072, 3072], P('kv'), may hold values from -0.15625 to 0.15625
- channel_gain: float32 [3072], replicated, may hold values from 0.1 to 1.9
- w_gate: bfloat16 [3072, 8448], P(None, 'kv'), may hold values from -0.109375 to 0.109375
- w_up: bfloat16 [3072, 8448], P(None, 'kv'), may hold values from -0.109375 to 0.109375
- w_down: bfloat16 [8448, 3072], P(None, 'kv'), may hold values from -0.0625 to 0.0625
Outputs:
- mixed: bfloat16 [32, 3072], P(('tp', 'dp'), 'kv'), parts along dimension 0
- new_state: float32 [32, 24, 128, 128], P(('tp', 'dp', 'kv')), parts along dimension 0
There are 2 independent parts, one for each index of `tp`. A program takes and returns all parts, laid end to end along the dimension named above; an argument that names none is the same for every part. Nothing has to cross between parts.
All inputs are finite; a program needn't handle non-finite values.
Results may differ from a plain program's by a relative error of at most 0.0059.
Values may be sent and summed in bfloat16 or wider, within the bound.
A program may use at most 64 MiB of HBM per device.

v0:
```python
import jax
import jax.numpy as jnp
from jax import lax
from jax.sharding import PartitionSpec as P

HEADS = 24
HEAD_DIM = 128
EPS = 1e-06


def norm_scale(values):
    return lax.rsqrt(jnp.mean(values * values, axis=-1, keepdims=True) + EPS)


def unit_rows(values):
    return values * lax.rsqrt(jnp.sum(values * values, axis=-1, keepdims=True) + EPS)


def body(
    tokens,
    old_state,
    mixer_gain,
    w_query,
    w_key,
    w_value,
    w_outgate,
    w_decay,
    w_write,
    decay_log,
    decay_bias,
    head_gain,
    w_output,
    channel_gain,
    w_gate,
    w_up,
    w_down,
):
    local_rows = old_state.shape[0]
    width_share = tokens.shape[1]
    offset_rows = lax.axis_index("kv") * local_rows
    offset_cols = lax.axis_index("kv") * width_share
    complete_rows = lax.all_gather(tokens, "kv", axis=1, tiled=True)
    tok_wide = complete_rows.astype(jnp.float32)
    scale_in = norm_scale(tok_wide)
    normed = (tok_wide * mixer_gain).astype(jnp.bfloat16)

    def project(weight):
        return (jnp.dot(normed, weight, preferred_element_type=jnp.float32) * scale_in).astype(
            jnp.bfloat16
        )

    query_cols = project(w_query)
    key_cols = project(w_key)
    value_cols = project(w_value)
    outgate_cols = project(w_outgate)
    query_pre, key_pre, value_pre, outgate_pre = (
        lax.all_to_all(query_cols, "kv", split_axis=0, concat_axis=1, tiled=True),
        lax.all_to_all(key_cols, "kv", split_axis=0, concat_axis=1, tiled=True),
        lax.all_to_all(value_cols, "kv", split_axis=0, concat_axis=1, tiled=True),
        lax.all_to_all(outgate_cols, "kv", split_axis=0, concat_axis=1, tiled=True),
    )
    own_normed = lax.dynamic_slice_in_dim(normed, offset_rows, local_rows, 0)
    own_scale = lax.dynamic_slice_in_dim(scale_in, offset_rows, local_rows, 0)
    decay_pre = jnp.dot(own_normed, w_decay, preferred_element_type=jnp.float32) * own_scale
    write_pre = jnp.dot(own_normed, w_write, preferred_element_type=jnp.float32) * own_scale

    def by_head(values):
        return values.astype(jnp.float32).reshape(local_rows, HEADS, HEAD_DIM)

    queries = unit_rows(jax.nn.silu(by_head(query_pre))) * HEAD_DIM ** (-0.5)
    keys_unit = unit_rows(jax.nn.silu(by_head(key_pre)))
    values_act = jax.nn.silu(by_head(value_pre))
    strength = jax.nn.sigmoid(write_pre)
    retain = jnp.exp(-jnp.exp(decay_log) * jax.nn.softplus(decay_pre + decay_bias))
    recalled_values = jnp.einsum(
        "bhkv,bhk->bhv", old_state, keys_unit, precision=lax.Precision.HIGHEST
    )
    correction = values_act - retain[..., None] * recalled_values
    new_state = (
        retain[..., None, None] * old_state
        + (strength[..., None] * keys_unit)[..., :, None] * correction[..., None, :]
    )
    state_readout = jnp.einsum("bhkv,bhk->bhv", new_state, queries, precision=lax.Precision.HIGHEST)
    gated_read = (
        state_readout * norm_scale(state_readout) * head_gain * jax.nn.silu(by_head(outgate_pre))
    )
    gated_read = gated_read.reshape(local_rows, HEADS * HEAD_DIM).astype(jnp.bfloat16)
    read_cols = lax.all_to_all(gated_read, "kv", split_axis=1, concat_axis=0, tiled=True)
    partial_out = jnp.dot(read_cols, w_output, preferred_element_type=jnp.float32)
    mixer_out = lax.psum(partial_out, "kv")
    residual = lax.optimization_barrier((tok_wide + mixer_out).astype(jnp.bfloat16))
    residual_wide = residual.astype(jnp.float32)
    scale_mid = norm_scale(residual_wide)
    normed_mid = (residual_wide * channel_gain).astype(jnp.bfloat16)
    gate_act = jnp.dot(normed_mid, w_gate, preferred_element_type=jnp.float32) * scale_mid
    upward = jnp.dot(normed_mid, w_up, preferred_element_type=jnp.float32) * scale_mid
    own_residual = lax.dynamic_slice_in_dim(residual_wide, offset_cols, width_share, 1)
    hidden_units = (jax.nn.silu(gate_act) * upward).astype(jnp.bfloat16)
    down_sum = jnp.dot(
        lax.all_gather(hidden_units, "kv", axis=1, tiled=True),
        w_down,
        preferred_element_type=jnp.float32,
    )
    mixed = (own_residual + down_sum).astype(jnp.bfloat16)
    return (mixed, new_state)


def solution(mesh):
    in_specs = (
        P(("tp", "dp"), "kv"),
        P(("tp", "dp", "kv"), None, None, None),
        P(),
        P(None, "kv"),
        P(None, "kv"),
        P(None, "kv"),
        P(None, "kv"),
        P(),
        P(),
        P(),
        P(),
        P(),
        P("kv", None),
        P(),
        P(None, "kv"),
        P(None, "kv"),
        P(None, "kv"),
    )
    out_specs = (P(("tp", "dp"), "kv"), P(("tp", "dp", "kv"), None, None, None))
    return jax.shard_map(body, mesh=mesh, in_specs=in_specs, out_specs=out_specs, check_vma=False)
```

profile of v0, /device:TPU:0, one launch (start us, length us, event | category | flops | bytes accessed | tf_op | source)
XLA Modules:
  0.0 226.5 jit_solution(14168076446692269067)
XLA Ops:
  7.2 32.9 %all_gather.6 = bf16[8,3072]{1,0:T(8,128)(2,1)S(1)} all-gather(bf16[8,384]{1,0:T(8,128)(2,1)} %param.17), channel_id=1, replica_groups=mesh['dp'=2,'kv'=8,'tp'=2] {'kv'}, dimensions={1}, use_global_device_ids=true | all-gather | bytes 55296 | tf_op jit(solution)/shard_map/all_gather | solution.py:42
  40.1 0.8 fusion.24
  41.0 2.1 fusion.15
  43.0 0.5 broadcast.215
  43.6 0.6 reduce.6
  44.2 0.7 reshape.400
  44.9 5.4 %all-to-all-start = ((bf16[8,2,192]{2,1,0:T(2,128)(2,1)}), bf16[8,2,192]{2,1,0:T(2,128)(2,1)S(1)}, u32[]{:S(2)}, u32[]{:S(2)}) async-start(bf16[8,2,192]{2,1,0:T(2,128)(2,1)} %reshape.400), calls=%async_computation | async-start | bytes 16384 | tf_op jit(solution)/shard_map/all_to_all | solution.py:58
  50.3 0.6 dynamic-slice.3
  50.9 2.2 fusion.14
  53.1 0.4 fusion.13
  53.6 0.4 fusion.12
  54.0 0.1 copy-done.5
  54.1 0.8 fusion.46
  54.9 0.8 fusion.20
  55.7 0.7 reduce.7
  56.4 0.7 reshape.402
  57.1 0.6 reduce.5
  57.8 0.7 reshape.398
  58.4 0.6 reduce.4
  59.1 0.7 reshape.396
  59.8 6.0 %all-to-all-start.1 = ((bf16[8,2,192]{2,1,0:T(2,128)(2,1)}), bf16[8,2,192]{2,1,0:T(2,128)(2,1)S(1)}, u32[]{:S(2)}, u32[]{:S(2)}) async-start(bf16[8,2,192]{2,1,0:T(2,128)(2,1)} %reshape.402), calls=%async_computation.1 | async-start | bytes 16384 | tf_op jit(solution)/shard_map/all_to_all | solution.py:59
  65.8 0.1 reshape.401
  65.9 0.1 fusion.36
  66.0 6.3 %all-to-all-done.1 = bf16[8,2,192]{2,1,0:T(2,128)(2,1)S(1)} async-done(((bf16[8,2,192]{2,1,0:T(2,128)(2,1)}), bf16[8,2,192]{2,1,0:T(2,128)(2,1)S(1)}, u32[]{:S(2)}, u32[]{:S(2)}) %all-to-all-start.1) | async-done | bytes 6176 | tf_op jit(solution)/shard_map/all_to_all | solution.py:59
  72.3 3.3 %all-to-all-start.2 = ((bf16[8,2,192]{2,1,0:T(2,128)(2,1)}), bf16[8,2,192]{2,1,0:T(2,128)(2,1)S(1)}, u32[]{:S(2)}, u32[]{:S(2)}) async-start(bf16[8,2,192]{2,1,0:T(2,128)(2,1)} %reshape.398), calls=%async_computation.2 | async-start | bytes 16384 | tf_op jit(solution)/shard_map/all_to_all | solution.py:57
  75.6 0.1 reshape.403
  75.8 6.3 %all-to-all-done.2 = bf16[8,2,192]{2,1,0:T(2,128)(2,1)S(1)} async-done(((bf16[8,2,192]{2,1,0:T(2,128)(2,1)}), bf16[8,2,192]{2,1,0:T(2,128)(2,1)S(1)}, u32[]{:S(2)}, u32[]{:S(2)}) %all-to-all-start.2) | async-done | bytes 6176 | tf_op jit(solution)/shard_map/all_to_all | solution.py:57
  82.1 3.3 %all-to-all-start.3 = ((bf16[8,2,192]{2,1,0:T(2,128)(2,1)}), bf16[8,2,192]{2,1,0:T(2,128)(2,1)S(1)}, u32[]{:S(2)}, u32[]{:S(2)}) async-start(bf16[8,2,192]{2,1,0:T(2,128)(2,1)} %reshape.396), calls=%async_computation.3 | async-start | bytes 16384 | tf_op jit(solution)/shard_map/all_to_all | solution.py:60
  85.5 0.1 reshape.399
  85.6 0.1 fusion.37
  85.8 2.9 %fusion.5 = f32[24,1,128]{2,1,0:T(1,128)S(1)} fusion(f32[24,128,1]{1,2,0:T(1,128)S(1)} %bitcast.127, f32[1,24,128,128]{3,2,1,0:T(8,128)} %param.18), kind=kOutput, calls=%fused_computation.7 | convolution fusion | flops 4718592 | bytes 1597440 | tf_op jit(solution)/shard_map/bhkv,bhk->bhv/dot_general | solution.py:75
  88.8 0.6 multiply_add_fusion
  89.5 1.1 copy-done.2
  90.5 1.4 fusion.3
  92.0 0.1 multiply_reduce_fusion.1
  92.1 0.1 reshape.397
  92.3 0.7 reduce.8
  93.1 12.2 %all_to_all.65 = bf16[8,2,192]{2,1,0:T(2,128)(2,1)S(1)} all-to-all(bf16[8,2,192]{2,1,0:T(2,128)(2,1)S(1)} %reshape.404), channel_id=1, replica_groups=mesh['dp'=2,'kv'=8,'tp'=2] {'kv'}, dimensions={0} | all-to-all | bytes 12288 | tf_op jit(solution)/shard_map/all_to_all | solution.py:88
  105.3 0.1 reshape.405
  105.4 1.1 fusion.40
  106.5 67.6 %all-reduce.2.cloned.1.call-done = f32[8,3072]{1,0:T(8,128)} async-done(((f32[8,3072]{1,0:T(8,128)}), f32[8,3072]{1,0:T(8,128)}) %all-reduce.2.cloned.1.call-update) | async-done | bytes 98320 | tf_op jit(solution)/shard_map/psum | solution.py:90
  174.1 0.9 fusion.25
  175.0 0.1 multiply_reduce_fusion
  175.2 4.6 %convolution_multiply_fusion.1 = f32[8,1056]{1,0:T(8,128)S(1)} fusion(bf16[3072,1056]{0,1:T(8,128)(2,1)} %param.31, f32[3072]{0:T(1024)S(1)} %copy-done.7, bf16[8,3072]{1,0:T(8,128)(2,1)S(1)} %fusion.25, f32[8]{0:T(128)S(1)} %add_rsqrt_fusion), kind=kOutput, calls=%fused_computation.2 | convolution fusion | flops 51986688 | bytes 6583328 | tf_op jit(solution)/shard_map/dot_general | solution.py:95
  179.8 4.6 %fusion.2 = bf16[1,1056,8]{1,2,0:T(8,128)(2,1)S(1)} fusion(bf16[3072,1056]{0,1:T(8,128)(2,1)} %param.32, f32[3072]{0:T(1024)S(1)} %copy-done.7, bf16[8,3072]{1,0:T(8,128)(2,1)S(1)} %fusion.25, f32[8,1056]{1,0:T(8,128)S(1)} %convolution_multiply_fusion.1, f32[8]{0:T(128)S(1)} %add_rsqrt_fusion), kind=kOutput, calls=%fused_computation.4 | convolution fusion | flops 52037376 | bytes 6600224 | tf_op jit(solution)/shard_map/dot_general | solution.py:96
  184.4 30.7 %all-gather = bf16[8,1056,8]{1,2,0:T(8,128)(2,1)S(1)} all-gather(bf16[1,1056,8]{1,2,0:T(8,128)(2,1)S(1)} %fusion.2), channel_id=1, replica_groups=mesh['dp'=2,'kv'=8,'tp'=2] {'kv'}, dimensions={0}, use_global_device_ids=true | all-gather | bytes 152064 | tf_op jit(solution)/shard_map/all_gather | solution.py:100
  215.1 0.1 reshape.385
  215.3 4.4 %fusion.11 = bf16[8,384]{1,0:T(8,128)(2,1)} fusion(bf16[8448,8]{0,1:T(8,128)(2,1)S(1)} %reshape.385, bf16[8448,384]{1,0:T(8,128)(2,1)} %param.33, f32[8,3072]{1,0:T(8,128)S(1)} %convert_element_type.150, s32[]{:T(128)S(6)} %select_n.14), kind=kOutput, calls=%fused_computation.19 | convolution fusion | flops 51910656 | bytes 6641668 | tf_op jit(solution)/shard_map/dot_general | solution.py:99
  (41 shorter events, 0.6 us)
Async XLA Ops:
  7.2 98.2 %copy-start = (bf16[384,3072]{1,0:T(8,128)(2,1)S(1)}, bf16[384,3072]{1,0:T(8,128)(2,1)}, u32[]{:S(2)}) copy-start(bf16[384,3072]{1,0:T(8,128)(2,1)} %param.29) | copy-start | bytes 7077892
  44.9 14.9 %all-to-all-start = ((bf16[8,2,192]{2,1,0:T(2,128)(2,1)}), bf16[8,2,192]{2,1,0:T(2,128)(2,1)S(1)}, u32[]{:S(2)}, u32[]{:S(2)}) async-start(bf16[8,2,192]{2,1,0:T(2,128)(2,1)} %reshape.400), calls=%async_computation | async-start | bytes 16384 | tf_op jit(solution)/shard_map/all_to_all | solution.py:58
  50.3 2.8 %copy-start.3 = (bf16[3072,384]{1,0:T(8,128)(2,1)S(1)}, bf16[3072,384]{1,0:T(8,128)(2,1)}, u32[]{:S(2)}) copy-start(bf16[3072,384]{1,0:T(8,128)(2,1)} %param.20) | copy-start | bytes 7077892
  50.9 2.7 %copy-start.4 = (bf16[3072,384]{1,0:T(8,128)(2,1)S(1)}, bf16[3072,384]{1,0:T(8,128)(2,1)}, u32[]{:S(2)}) copy-start(bf16[3072,384]{1,0:T(8,128)(2,1)} %param.23) | copy-start | bytes 7077892
  53.1 1.0 copy-start.5
  53.1 1.0 copy-start.8
  53.1 1.0 copy-start.9
  53.1 1.8 copy-start.6
  59.8 12.5 %all-to-all-start.1 = ((bf16[8,2,192]{2,1,0:T(2,128)(2,1)}), bf16[8,2,192]{2,1,0:T(2,128)(2,1)S(1)}, u32[]{:S(2)}, u32[]{:S(2)}) async-start(bf16[8,2,192]{2,1,0:T(2,128)(2,1)} %reshape.402), calls=%async_computation.1 | async-start | bytes 16384 | tf_op jit(solution)/shard_map/all_to_all | solution.py:59
  72.3 9.8 %all-to-all-start.2 = ((bf16[8,2,192]{2,1,0:T(2,128)(2,1)}), bf16[8,2,192]{2,1,0:T(2,128)(2,1)S(1)}, u32[]{:S(2)}, u32[]{:S(2)}) async-start(bf16[8,2,192]{2,1,0:T(2,128)(2,1)} %reshape.398), calls=%async_computation.2 | async-start | bytes 16384 | tf_op jit(solution)/shard_map/all_to_all | solution.py:57
  82.1 10.0 %all-to-all-start.3 = ((bf16[8,2,192]{2,1,0:T(2,128)(2,1)}), bf16[8,2,192]{2,1,0:T(2,128)(2,1)S(1)}, u32[]{:S(2)}, u32[]{:S(2)}) async-start(bf16[8,2,192]{2,1,0:T(2,128)(2,1)} %reshape.396), calls=%async_computation.3 | async-start | bytes 16384 | tf_op jit(solution)/shard_map/all_to_all | solution.py:60
  85.4 88.6 %all-reduce.2.cloned.1.call-start = ((), (), s32[]{:S(2)}) async-start(), calls=%async_computation.5 | async-start | bytes 196608 | tf_op jit(solution)/shard_map/psum | solution.py:90
  85.6 3.2 %copy-start.1 = (f32[1,24,128,128]{3,2,1,0:T(8,128)S(1)}, f32[1,24,128,128]{3,2,1,0:T(8,128)}, u32[]{:S(2)}) copy-start(f32[1,24,128,128]{3,2,1,0:T(8,128)} %param.18) | copy-start | bytes 4718596
  88.8 3.4 %copy-start.10 = (f32[128]{0:T(128)S(1)}, f32[128]{0:T(128)}, u32[]{:S(2)}) copy-start(f32[128]{0:T(128)} %param.28) | copy-start | bytes 1540
  89.4 1.1 copy-start.2
  90.5 84.6 %copy-start.7 = (f32[3072]{0:T(1024)S(1)}, f32[3072]{0:T(1024)}, u32[]{:S(2)}) copy-start(f32[3072]{0:T(1024)} %param.30) | copy-start | bytes 36868
Sparse Core Ops, SparseCore 0:
  106.6 67.4 all-reduce.1
where the time goes:
time: 227 us
  waiting for transfers between devices  80.3 us (35%)
  blocking collectives  75.8 us (33%)
  matrix products  25.8 us (11%)
  starting transfers between devices  18.1 us (8%)
  between operations  14.3 us (6%)
  other arithmetic  6.49 us (3%)
  local copies, waits for them, and re-layouts  5.82 us (3%)
    psum x1, waiting for transfers between devices, body(): mixer_out = lax.psum(partial_out, 'kv')  67.6 us
    all_gather x1, blocking collectives, body(): complete_rows = lax.all_gather(tokens, 'kv', axis=1, tiled=True)  32.9 us
    all_gather x1, blocking collectives, body(): lax.all_gather(hidden_units, 'kv', axis=1, tiled=True)  30.7 us
    all_to_all x1, blocking collectives, body(): lax.all_to_all(gated_read, 'kv', split_axis=1, concat_axis=0, tiled=True)  12.2 us
    all_to_all x1, waiting for transfers between devices, body(): lax.all_to_all(query_cols, 'kv', split_axis=0, concat_axis=1, tiled=True)  6.33 us
    all_to_all x1, waiting for transfers between devices, body(): lax.all_to_all(value_cols, 'kv', split_axis=0, concat_axis=1, tiled=True)  6.29 us
    all_to_all x1, starting transfers between devices, body(): lax.all_to_all(value_cols, 'kv', split_axis=0, concat_axis=1, tiled=True)  5.99 us
    all_to_all x1, starting transfers between devices, body(): lax.all_to_all(key_cols, 'kv', split_axis=0, concat_axis=1, tiled=True)  5.36 us
  transfers between devices with their start and end apart: 5, of which 3 were waited for; matrix products, arithmetic and copies ran while one was open for 7% of the time, Pallas kernels for 0%

commit v1 on v0

--- a/solution.py
+++ b/solution.py
@@ -87,7 +87,7 @@
     gated_read = gated_read.reshape(local_rows, HEADS * HEAD_DIM).astype(jnp.bfloat16)
     read_cols = lax.all_to_all(gated_read, "kv", split_axis=1, concat_axis=0, tiled=True)
     partial_out = jnp.dot(read_cols, w_output, preferred_element_type=jnp.float32)
-    mixer_out = lax.psum(partial_out, "kv")
+    mixer_out = jnp.sum(lax.all_gather(partial_out, "kv"), axis=0)
     residual = lax.optimization_barrier((tok_wide + mixer_out).astype(jnp.bfloat16))
     residual_wide = residual.astype(jnp.float32)
     scale_mid = norm_scale(residual_wide)

time: 227 us -> 181 us (0.80)
  waiting for transfers between devices: 80.3 us -> 25.3 us
  blocking collectives: 75.8 us -> 95.9 us
  between operations: 14.3 us -> 0.91 us
  starting transfers between devices: 18.1 us -> 21.3 us
    psum x1 -> x0, waiting for transfers between devices: 67.6 us -> none  [body(): mixer_out = lax.psum(partial_out, 'kv')]
    all_gather x0 -> x1, blocking collectives: none -> 32.4 us  [body(): mixer_out = jnp.sum(lax.all_gather(partial_out, 'kv'), axis=0)]
    all_to_all x1 -> x0, blocking collectives: 12.2 us -> none  [body(): lax.all_to_all(gated_read, 'kv', split_axis=1, concat_axis=0, tiled=True)]
    all_to_all x0 -> x1, waiting for transfers between devices: none -> 6.46 us  [body(): lax.all_to_all(gated_read, 'kv', split_axis=1, concat_axis=0, tiled=True)]
    all_to_all x1, waiting for transfers between devices: 0.01 us -> 6.22 us  [body(): lax.all_to_all(outgate_cols, 'kv', split_axis=0, concat_axis=1, tiled=True)]
    all_to_all x0 -> x1, starting transfers between devices: none -> 3.33 us  [body(): lax.all_to_all(gated_read, 'kv', split_axis=1, concat_axis=0, tiled=True)]
    all_to_all x1, starting transfers between devices: 5.99 us -> 3.33 us  [body(): lax.all_to_all(value_cols, 'kv', split_axis=0, concat_axis=1, tiled=True)]
    all_to_all x1, starting transfers between devices: 3.33 us -> 5.99 us  [body(): lax.all_to_all(query_cols, 'kv', split_axis=0, concat_axis=1, tiled=True)]
  transfers between devices with their start and end apart: 5 -> 5, of which waited for: 3 -> 4; matrix products, arithmetic and copies ran while one was open for 7% -> 5% of each run, Pallas kernels for 0% -> 0%
where the time goes in v1:
time: 181 us
  blocking collectives  95.9 us (53%)
  waiting for transfers between devices  25.3 us (14%)
  matrix products  25.1 us (14%)
  starting transfers between devices  21.3 us (12%)
  local copies, waits for them, and re-layouts  6.48 us (4%)
  other arithmetic  5.64 us (3%)
    all_gather x1, blocking collectives, body(): complete_rows = lax.all_gather(tokens, 'kv', axis=1, tiled=True)  32.9 us
    all_gather x1, blocking collectives, body(): mixer_out = jnp.sum(lax.all_gather(partial_out, 'kv'), axis=0)  32.4 us
    all_gather x1, blocking collectives, body(): lax.all_gather(hidden_units, 'kv', axis=1, tiled=True)  30.6 us
    all_to_all x1, waiting for transfers between devices, body(): lax.all_to_all(gated_read, 'kv', split_axis=1, concat_axis=0, tiled=True)  6.46 us
    all_to_all x1, waiting for transfers between devices, body(): lax.all_to_all(value_cols, 'kv', split_axis=0, concat_axis=1, tiled=True)  6.33 us
    all_to_all x1, waiting for transfers between devices, body(): lax.all_to_all(query_cols, 'kv', split_axis=0, concat_axis=1, tiled=True)  6.28 us
    all_to_all x1, waiting for transfers between devices, body(): lax.all_to_all(outgate_cols, 'kv', split_axis=0, concat_axis=1, tiled=True)  6.22 us
    all_to_all x1, starting transfers between devices, body(): lax.all_to_all(query_cols, 'kv', split_axis=0, concat_axis=1, tiled=True)  5.99 us
  transfers between devices with their start and end apart: 5, of which 4 were waited for; matrix products, arithmetic and copies ran while one was open for 5% of the time, Pallas kernels for 0%

profile of v1, /device:TPU:0, one launch (start us, length us, event | category | flops | bytes accessed | tf_op | source)
XLA Modules:
  0.0 180.7 jit_solution(4412473345242781262)
XLA Ops:
  0.6 32.9 %all_gather.12 = bf16[8,3072]{1,0:T(8,128)(2,1)S(1)} all-gather(bf16[8,384]{1,0:T(8,128)(2,1)} %param.17), channel_id=1, replica_groups=mesh['dp'=2,'kv'=8,'tp'=2] {'kv'}, dimensions={1}, use_global_device_ids=true | all-gather | bytes 55296 | tf_op jit(solution)/shard_map/all_gather | solution.py:42
  33.6 0.8 fusion.24
  34.4 2.1 %fusion.15 = bf16[8,1,384]{2,0,1:T(8,128)(2,1)S(1)} fusion(bf16[8,3072]{1,0:T(8,128)(2,1)S(1)} %get-tuple-element.5, bf16[3072,384]{1,0:T(8,128)(2,1)} %param.21, f32[8]{0:T(128)S(1)} %add_rsqrt_fusion.4), kind=kOutput, calls=%fused_computation.23 | convolution fusion | flops 18880512 | bytes 2414624 | tf_op jit(solution)/shard_map/dot_general | solution.py:48
  36.5 0.5 broadcast.215
  37.0 0.6 reduce.6
  37.7 0.7 reshape.401
  38.4 5.4 %all-to-all-start = ((bf16[8,2,192]{2,1,0:T(2,128)(2,1)}), bf16[8,2,192]{2,1,0:T(2,128)(2,1)S(1)}, u32[]{:S(2)}, u32[]{:S(2)}) async-start(bf16[8,2,192]{2,1,0:T(2,128)(2,1)} %reshape.401), calls=%async_computation | async-start | bytes 16384 | tf_op jit(solution)/shard_map/all_to_all | solution.py:58
  43.7 0.6 dynamic-slice.3
  44.3 2.2 %fusion.14 = bf16[8,1,384]{2,0,1:T(8,128)(2,1)S(1)} fusion(bf16[8,3072]{1,0:T(8,128)(2,1)S(1)} %get-tuple-element.5, bf16[3072,384]{1,0:T(8,128)(2,1)} %param.22, f32[8]{0:T(128)S(1)} %add_rsqrt_fusion.4), kind=kOutput, calls=%fused_computation.22 | convolution fusion | flops 18880512 | bytes 2414624 | tf_op jit(solution)/shard_map/dot_general | solution.py:48
  46.6 0.4 fusion.13
  47.0 0.4 fusion.12
  47.4 0.1 copy-done.5
  47.6 0.8 fusion.46
  48.4 0.8 fusion.20
  49.2 0.7 reduce.7
  49.9 0.7 reshape.403
  50.6 0.6 reduce.5
  51.2 0.7 reshape.399
  51.9 0.6 reduce.4
  52.6 0.7 reshape.397
  53.2 6.0 %all-to-all-start.2 = ((bf16[8,2,192]{2,1,0:T(2,128)(2,1)}), bf16[8,2,192]{2,1,0:T(2,128)(2,1)S(1)}, u32[]{:S(2)}, u32[]{:S(2)}) async-start(bf16[8,2,192]{2,1,0:T(2,128)(2,1)} %reshape.399), calls=%async_computation.2 | async-start | bytes 16384 | tf_op jit(solution)/shard_map/all_to_all | solution.py:57
  59.2 0.1 reshape.402
  59.4 0.1 fusion.36
  59.5 6.3 %all-to-all-done.2 = bf16[8,2,192]{2,1,0:T(2,128)(2,1)S(1)} async-done(((bf16[8,2,192]{2,1,0:T(2,128)(2,1)}), bf16[8,2,192]{2,1,0:T(2,128)(2,1)S(1)}, u32[]{:S(2)}, u32[]{:S(2)}) %all-to-all-start.2) | async-done | bytes 6176 | tf_op jit(solution)/shard_map/all_to_all | solution.py:57
  65.8 3.3 %all-to-all-start.3 = ((bf16[8,2,192]{2,1,0:T(2,128)(2,1)}), bf16[8,2,192]{2,1,0:T(2,128)(2,1)S(1)}, u32[]{:S(2)}, u32[]{:S(2)}) async-start(bf16[8,2,192]{2,1,0:T(2,128)(2,1)} %reshape.397), calls=%async_computation.3 | async-start | bytes 16384 | tf_op jit(solution)/shard_map/all_to_all | solution.py:60
  69.1 0.1 reshape.400
  69.2 0.1 fusion.37
  69.3 6.2 %all-to-all-done.3 = bf16[8,2,192]{2,1,0:T(2,128)(2,1)S(1)} async-done(((bf16[8,2,192]{2,1,0:T(2,128)(2,1)}), bf16[8,2,192]{2,1,0:T(2,128)(2,1)S(1)}, u32[]{:S(2)}, u32[]{:S(2)}) %all-to-all-start.3) | async-done | bytes 6176 | tf_op jit(solution)/shard_map/all_to_all | solution.py:60
  75.6 3.3 %all-to-all-start.1 = ((bf16[8,2,192]{2,1,0:T(2,128)(2,1)}), bf16[8,2,192]{2,1,0:T(2,128)(2,1)S(1)}, u32[]{:S(2)}, u32[]{:S(2)}) async-start(bf16[8,2,192]{2,1,0:T(2,128)(2,1)} %reshape.403), calls=%async_computation.1 | async-start | bytes 16384 | tf_op jit(solution)/shard_map/all_to_all | solution.py:59
  78.9 0.1 reshape.398
  79.0 6.3 %all-to-all-done.1 = bf16[8,2,192]{2,1,0:T(2,128)(2,1)S(1)} async-done(((bf16[8,2,192]{2,1,0:T(2,128)(2,1)}), bf16[8,2,192]{2,1,0:T(2,128)(2,1)S(1)}, u32[]{:S(2)}, u32[]{:S(2)}) %all-to-all-start.1) | async-done | bytes 6176 | tf_op jit(solution)/shard_map/all_to_all | solution.py:59
  85.6 2.9 %fusion.5 = f32[24,1,128]{2,1,0:T(1,128)S(1)} fusion(f32[24,128,1]{1,2,0:T(1,128)S(1)} %bitcast.129, f32[1,24,128,128]{3,2,1,0:T(8,128)} %param.18), kind=kOutput, calls=%fused_computation.7 | convolution fusion | flops 4718592 | bytes 1597440 | tf_op jit(solution)/shard_map/bhkv,bhk->bhv/dot_general | solution.py:75
  88.6 0.6 multiply_add_fusion
  89.2 1.1 copy-done.2
  90.3 1.4 fusion.3
  91.7 0.1 multiply_reduce_fusion.1
  92.0 0.7 reduce.8
  92.7 0.7 reshape.405
  93.4 3.3 %all-to-all-start.4 = ((bf16[8,2,192]{2,1,0:T(2,128)(2,1)}), bf16[8,2,192]{2,1,0:T(2,128)(2,1)S(1)}, u32[]{:S(2)}, u32[]{:S(2)}) async-start(bf16[8,2,192]{2,1,0:T(2,128)(2,1)} %reshape.405), calls=%async_computation.4 | async-start | bytes 16384 | tf_op jit(solution)/shard_map/all_to_all | solution.py:88
  96.7 6.5 %all-to-all-done.4 = bf16[8,2,192]{2,1,0:T(2,128)(2,1)S(1)} async-done(((bf16[8,2,192]{2,1,0:T(2,128)(2,1)}), bf16[8,2,192]{2,1,0:T(2,128)(2,1)S(1)}, u32[]{:S(2)}, u32[]{:S(2)}) %all-to-all-start.4) | async-done | bytes 6176 | tf_op jit(solution)/shard_map/all_to_all | solution.py:88
  103.3 0.4 fusion.40
  103.7 32.4 %all-gather = f32[64,3072]{1,0:T(8,128)S(1)} all-gather(f32[8,3072]{1,0:T(8,128)S(1)} %fusion.40), channel_id=2, replica_groups=mesh['dp'=2,'kv'=8,'tp'=2] {'kv'}, dimensions={0}, use_global_device_ids=true | all-gather | bytes 884736 | tf_op jit(solution)/shard_map/all_gather | solution.py:90
  136.1 0.1 multiply_reduce_fusion
  136.3 4.6 %convolution_multiply_fusion.1 = f32[8,1056]{1,0:T(8,128)S(1)} fusion(bf16[3072,1056]{0,1:T(8,128)(2,1)} %param.31, f32[3072]{0:T(1024)S(1)} %copy-done.7, bf16[8,3072]{1,0:T(8,128)(2,1)S(1)} %fusion.25, f32[8]{0:T(128)S(1)} %add_rsqrt_fusion), kind=kOutput, calls=%fused_computation.2 | convolution fusion | flops 51986688 | bytes 6583328 | tf_op jit(solution)/shard_map/dot_general | solution.py:95
  140.9 4.6 %fusion.2 = bf16[1,1056,8]{1,2,0:T(8,128)(2,1)S(1)} fusion(bf16[3072,1056]{0,1:T(8,128)(2,1)} %param.32, f32[3072]{0:T(1024)S(1)} %copy-done.7, bf16[8,3072]{1,0:T(8,128)(2,1)S(1)} %fusion.25, f32[8,1056]{1,0:T(8,128)S(1)} %convolution_multiply_fusion.1, f32[8]{0:T(128)S(1)} %add_rsqrt_fusion), kind=kOutput, calls=%fused_computation.4 | convolution fusion | flops 52037376 | bytes 6600224 | tf_op jit(solution)/shard_map/dot_general | solution.py:96
  145.6 30.6 %all-gather.1 = bf16[8,1056,8]{1,2,0:T(8,128)(2,1)S(1)} all-gather(bf16[1,1056,8]{1,2,0:T(8,128)(2,1)S(1)} %fusion.2), channel_id=1, replica_groups=mesh['dp'=2,'kv'=8,'tp'=2] {'kv'}, dimensions={0}, use_global_device_ids=true | all-gather | bytes 152064 | tf_op jit(solution)/shard_map/all_gather | solution.py:100
  176.2 0.1 reshape.386
  176.3 4.4 %fusion.11 = bf16[8,384]{1,0:T(8,128)(2,1)} fusion(bf16[8448,8]{0,1:T(8,128)(2,1)S(1)} %reshape.386, bf16[8448,384]{1,0:T(8,128)(2,1)} %param.33, f32[8,3072]{1,0:T(8,128)S(1)} %convert_element_type.150, s32[]{:T(128)S(6)} %select_n.14), kind=kOutput, calls=%fused_computation.19 | convolution fusion | flops 51910656 | bytes 6641668 | tf_op jit(solution)/shard_map/dot_general | solution.py:99
  (41 shorter events, 0.7 us)
Async XLA Ops:
  0.6 102.6 %copy-start = (bf16[384,3072]{1,0:T(8,128)(2,1)S(1)}, bf16[384,3072]{1,0:T(8,128)(2,1)}, u32[]{:S(2)}) copy-start(bf16[384,3072]{1,0:T(8,128)(2,1)} %param.29) | copy-start | bytes 7077892
  38.4 14.9 %all-to-all-start = ((bf16[8,2,192]{2,1,0:T(2,128)(2,1)}), bf16[8,2,192]{2,1,0:T(2,128)(2,1)S(1)}, u32[]{:S(2)}, u32[]{:S(2)}) async-start(bf16[8,2,192]{2,1,0:T(2,128)(2,1)} %reshape.401), calls=%async_computation | async-start | bytes 16384 | tf_op jit(solution)/shard_map/all_to_all | solution.py:58
  43.7 2.8 %copy-start.3 = (bf16[3072,384]{1,0:T(8,128)(2,1)S(1)}, bf16[3072,384]{1,0:T(8,128)(2,1)}, u32[]{:S(2)}) copy-start(bf16[3072,384]{1,0:T(8,128)(2,1)} %param.20) | copy-start | bytes 7077892
  44.3 2.7 %copy-start.4 = (bf16[3072,384]{1,0:T(8,128)(2,1)S(1)}, bf16[3072,384]{1,0:T(8,128)(2,1)}, u32[]{:S(2)}) copy-start(bf16[3072,384]{1,0:T(8,128)(2,1)} %param.23) | copy-start | bytes 7077892
  46.6 1.0 copy-start.5
  46.6 1.0 copy-start.8
  46.6 1.0 copy-start.9
  46.6 1.8 copy-start.6
  53.2 12.5 %all-to-all-start.2 = ((bf16[8,2,192]{2,1,0:T(2,128)(2,1)}), bf16[8,2,192]{2,1,0:T(2,128)(2,1)S(1)}, u32[]{:S(2)}, u32[]{:S(2)}) async-start(bf16[8,2,192]{2,1,0:T(2,128)(2,1)} %reshape.399), calls=%async_computation.2 | async-start | bytes 16384 | tf_op jit(solution)/shard_map/all_to_all | solution.py:57
  65.8 9.8 %all-to-all-start.3 = ((bf16[8,2,192]{2,1,0:T(2,128)(2,1)}), bf16[8,2,192]{2,1,0:T(2,128)(2,1)S(1)}, u32[]{:S(2)}, u32[]{:S(2)}) async-start(bf16[8,2,192]{2,1,0:T(2,128)(2,1)} %reshape.397), calls=%async_computation.3 | async-start | bytes 16384 | tf_op jit(solution)/shard_map/all_to_all | solution.py:60
  75.6 9.8 %all-to-all-start.1 = ((bf16[8,2,192]{2,1,0:T(2,128)(2,1)}), bf16[8,2,192]{2,1,0:T(2,128)(2,1)S(1)}, u32[]{:S(2)}, u32[]{:S(2)}) async-start(bf16[8,2,192]{2,1,0:T(2,128)(2,1)} %reshape.403), calls=%async_computation.1 | async-start | bytes 16384 | tf_op jit(solution)/shard_map/all_to_all | solution.py:59
  85.5 3.1 %copy-start.1 = (f32[1,24,128,128]{3,2,1,0:T(8,128)S(1)}, f32[1,24,128,128]{3,2,1,0:T(8,128)}, u32[]{:S(2)}) copy-start(f32[1,24,128,128]{3,2,1,0:T(8,128)} %param.18) | copy-start | bytes 4718596
  88.6 3.3 %copy-start.10 = (f32[128]{0:T(128)S(1)}, f32[128]{0:T(128)}, u32[]{:S(2)}) copy-start(f32[128]{0:T(128)} %param.28) | copy-start | bytes 1540
  89.2 1.1 copy-start.2
  92.0 44.3 %copy-start.7 = (f32[3072]{0:T(1024)S(1)}, f32[3072]{0:T(1024)}, u32[]{:S(2)}) copy-start(f32[3072]{0:T(1024)} %param.30) | copy-start | bytes 36868
  93.4 9.8 %all-to-all-start.4 = ((bf16[8,2,192]{2,1,0:T(2,128)(2,1)}), bf16[8,2,192]{2,1,0:T(2,128)(2,1)S(1)}, u32[]{:S(2)}, u32[]{:S(2)}) async-start(bf16[8,2,192]{2,1,0:T(2,128)(2,1)} %reshape.405), calls=%async_computation.4 | async-start | bytes 16384 | tf_op jit(solution)/shard_map/all_to_all | solution.py:88
